TPU v7x, 32 devices: a whole 2x2x4 slice. The times are simulated.
32 devices in a mesh: sp: 8 (over z, x), tp: 4 (over y, core).
Axes of the slice: x: 2, y: 2, z: 4, core: 2. Of those that a mesh axis runs over, the one named last changes fastest.
Arguments:
- queries: bfloat16 [4096, 2048], P('sp', 'tp'), may hold values from -4.5 to 4.5
- keys: bfloat16 [4096, 2048], P('sp', 'tp'), may hold values from -4.5 to 4.5
- values: bfloat16 [4096, 2048], P('sp', 'tp'), may hold values from -6 to 6
- forget_logits: float32 [4096, 16], P('sp', 'tp'), may hold values from -1 to 20
- layer_input: bfloat16 [4096, 4096], P('sp', 'tp'), may hold values from -0.125 to 0.125
- out_grad: bfloat16 [4096, 2048], P('sp', 'tp'), may hold values from -6 to 6
Outputs:
- query_grad: float32 [4096, 2048], P('sp', 'tp')
- key_grad: float32 [4096, 2048], P('sp', 'tp')
- value_grad: float32 [4096, 2048], P('sp', 'tp')
- weight_grad: float32 [4096, 2048], P('sp', 'tp')
All inputs are finite; a program needn't handle non-finite values.
Results may differ from a plain program's by a relative error of at most 0.04.
Values may be sent and summed in bfloat16 or wider, within the bound.
A program may use at most 64 MiB of HBM per device.

v0:
```python
import jax
import jax.numpy as jnp
from jax import lax
from jax.sharding import PartitionSpec as P

HEAD = 128


neg_big = -1e30


def block_rows(row_count, cap, unit):
    block_size = min(row_count, cap)
    while row_count % block_size != 0 or unit % block_size != 0:
        block_size -= 1
    return block_size


def attention_block(query_heads, query_bias, query_pos, key_heads, key_bias, key_pos):
    products = jnp.einsum(
        "qhd,khd->hqk", query_heads, key_heads, preferred_element_type=jnp.float32
    )
    scores = products * HEAD ** (-0.5) + query_bias.T[:, :, None] - key_bias.T[:, None, :]
    visible = key_pos[None, :] <= query_pos[:, None]
    return (scores, visible[None])


def local(queries, keys, values, forget_logits, layer_input, out_grad):
    local_rows = queries.shape[0]
    head_count = queries.shape[1] // HEAD
    score_scale = HEAD ** (-0.5)
    shards = lax.axis_size("sp")
    all_rows = local_rows * shards
    my_index = lax.axis_index("sp")
    groups = ((0, local_rows, my_index * local_rows),)
    block_cap = 512
    local_gates = jnp.cumsum(jax.nn.log_sigmoid(forget_logits), axis=0)
    gathered_gates = lax.all_gather(local_gates, "sp", axis=0, tiled=True)
    per_shard = gathered_gates.reshape(shards, local_rows, head_count)
    shard_totals = per_shard[:, -1, :]
    before = jnp.concatenate(
        [jnp.zeros((1, head_count), jnp.float32), jnp.cumsum(shard_totals, axis=0)[:-1]], axis=0
    )
    bias_all = (per_shard + before[:, None, :]).reshape(all_rows, head_count)
    query_heads = queries.reshape(local_rows, head_count, HEAD)
    grad_heads = out_grad.reshape(local_rows, head_count, HEAD)
    key_local = keys.reshape(local_rows, head_count, HEAD)
    value_local = values.reshape(local_rows, head_count, HEAD)
    group_data = []
    lower, count, start = groups[0]
    group_data.append(
        (
            query_heads,
            grad_heads,
            key_local,
            value_local,
            lax.dynamic_slice_in_dim(bias_all, start, count, 0),
            start + jnp.arange(count, dtype=jnp.int32),
        )
    )

    def for_blocks(current, pieces, visitor):
        row_count = pieces[0].shape[0]
        block_size = block_rows(row_count, block_cap, local_rows)
        stacked = tuple(
            (
                piece.reshape((row_count // block_size, block_size) + piece.shape[1:])
                for piece in pieces
            )
        )

        def one_block(state, inputs):
            number, block_parts = inputs
            return (visitor(state, block_parts, number * block_size), None)

        numbers = jnp.arange(row_count // block_size, dtype=jnp.int32)
        current, _ = lax.scan(one_block, current, (numbers, stacked))
        return current

    def keep_state(state):
        return state

    def forward_visit(current, block_parts, begin_at):
        key_part, value_part = block_parts
        block_size = key_part.shape[0]
        key_heads = key_part.reshape(block_size, head_count, HEAD)
        value_heads = value_part.reshape(block_size, head_count, HEAD)
        key_bias = lax.dynamic_slice_in_dim(bias_all, begin_at, block_size, 0)
        key_pos = begin_at + jnp.arange(block_size, dtype=jnp.int32)
        results = []
        for number, (lower, count, start) in enumerate(groups):
            group_query, _, _, _, group_bias, group_pos = group_data[number]

            def update(state, group_query=group_query, group_bias=group_bias, group_pos=group_pos):
                highest, weight_sum, weighted = state
                scores, visible = attention_block(
                    group_query, group_bias, group_pos, key_heads, key_bias, key_pos
                )
                new_high = jnp.maximum(
                    highest, jnp.max(jnp.where(visible, scores, neg_big), axis=2)
                )
                weights = jnp.where(visible, jnp.exp(scores - new_high[:, :, None]), 0.0)
                shrink = jnp.exp(highest - new_high)
                weight_sum = weight_sum * shrink + jnp.sum(weights, axis=2)
                mixed_values = jnp.einsum(
                    "hqk,khd->qhd",
                    weights.astype(jnp.bfloat16),
                    value_heads,
                    preferred_element_type=jnp.float32,
                )
                weighted = weighted * shrink.T[:, :, None] + mixed_values
                return (new_high, weight_sum, weighted)

            results.append(
                lax.cond(begin_at <= start + count - 1, update, keep_state, current[number])
            )
        return tuple(results)

    start_state = tuple(
        (
            (
                jnp.full((head_count, count), neg_big, jnp.float32),
                jnp.zeros((head_count, count), jnp.float32),
                jnp.zeros((count, head_count, HEAD), jnp.float32),
            )
            for lower, count, start in groups
        )
    )
    forward_state = for_blocks(
        start_state,
        (
            lax.all_gather(keys, "sp", axis=0, tiled=True),
            lax.all_gather(values, "sp", axis=0, tiled=True),
        ),
        forward_visit,
    )
    highest = jnp.concatenate([state[0] for state in forward_state], axis=1)
    weight_sum = jnp.concatenate([state[1] for state in forward_state], axis=1)
    weighted = jnp.concatenate([state[2] for state in forward_state], axis=0)
    lse_heads = highest + jnp.log(weight_sum)
    attended = (weighted / weight_sum.T[:, :, None]).astype(jnp.bfloat16)
    row_terms = jnp.sum(attended.astype(jnp.float32) * grad_heads.astype(jnp.float32), axis=2)
    term_heads = row_terms.T
    lse_rows = lse_heads.T

    def key_side_visit():

        def visitor(current, block_parts, begin_at):
            key_part, value_part = block_parts
            block_size = key_part.shape[0]
            key_heads = key_part.reshape(block_size, head_count, HEAD)
            value_heads = value_part.reshape(block_size, head_count, HEAD)
            key_bias = lax.dynamic_slice_in_dim(bias_all, begin_at, block_size, 0)
            key_pos = begin_at + jnp.arange(block_size, dtype=jnp.int32)
            query_parts = list(current[0])
            key_sum = jnp.zeros((block_size, head_count, HEAD), jnp.float32)
            value_sum = jnp.zeros((block_size, head_count, HEAD), jnp.float32)
            for number, (lower, count, start) in enumerate(groups):
                group_query, group_grad, _, _, group_bias, group_pos = group_data[number]
                group_lse = lse_heads
                group_terms = term_heads

                def update(
                    state,
                    group_query=group_query,
                    group_grad=group_grad,
                    group_bias=group_bias,
                    group_pos=group_pos,
                    group_lse=group_lse,
                    group_terms=group_terms,
                ):
                    query_part, key_acc, value_acc = state
                    scores, visible = attention_block(
                        group_query, group_bias, group_pos, key_heads, key_bias, key_pos
                    )
                    prob_rows = jnp.where(visible, jnp.exp(scores - group_lse[:, :, None]), 0.0)
                    prob_grad = jnp.einsum(
                        "qhd,khd->hqk", group_grad, value_heads, preferred_element_type=jnp.float32
                    )
                    score_grad = (prob_rows * (prob_grad - group_terms[:, :, None])).astype(
                        jnp.bfloat16
                    )
                    query_part = query_part + score_scale * jnp.einsum(
                        "hqk,khd->qhd", score_grad, key_heads, preferred_element_type=jnp.float32
                    )
                    return (query_part, key_acc, value_acc)

                query_parts[number], key_sum, value_sum = lax.cond(
                    begin_at <= start + count - 1,
                    update,
                    keep_state,
                    (query_parts[number], key_sum, value_sum),
                )
            return (tuple(query_parts),)

        return visitor

    def query_side_visit(lse_all, terms_all):

        def visitor(current, block_parts, begin_at):
            query_part, grad_part = block_parts
            block_size = query_part.shape[0]
            block_queries = query_part.reshape(block_size, head_count, HEAD)
            block_grads = grad_part.reshape(block_size, head_count, HEAD)
            block_bias = lax.dynamic_slice_in_dim(bias_all, begin_at, block_size, 0)
            block_pos = begin_at + jnp.arange(block_size, dtype=jnp.int32)
            block_lse = lax.dynamic_slice_in_dim(lse_all, begin_at, block_size, 0).T
            block_terms = lax.dynamic_slice_in_dim(terms_all, begin_at, block_size, 0).T
            key_parts = list(current[0])
            value_parts = list(current[1])
            query_sum = jnp.zeros((block_size, head_count, HEAD), jnp.float32)
            for number, (lower, count, start) in enumerate(groups):
                _, _, group_key, group_value, group_bias, group_pos = group_data[number]

                def update(
                    state,
                    group_key=group_key,
                    group_value=group_value,
                    group_bias=group_bias,
                    group_pos=group_pos,
                ):
                    key_acc, value_acc, query_acc = state
                    scores, visible = attention_block(
                        block_queries, block_bias, block_pos, group_key, group_bias, group_pos
                    )
                    prob_rows = jnp.where(visible, jnp.exp(scores - block_lse[:, :, None]), 0.0)
                    prob_grad = jnp.einsum(
                        "qhd,khd->hqk", block_grads, group_value, preferred_element_type=jnp.float32
                    )
                    score_grad = (prob_rows * (prob_grad - block_terms[:, :, None])).astype(
                        jnp.bfloat16
                    )
                    key_acc = key_acc + score_scale * jnp.einsum(
                        "hqk,qhd->khd",
                        score_grad,
                        block_queries,
                        preferred_element_type=jnp.float32,
                    )
                    value_acc = value_acc + jnp.einsum(
                        "hqk,qhd->khd",
                        prob_rows.astype(jnp.bfloat16),
                        block_grads,
                        preferred_element_type=jnp.float32,
                    )
                    return (key_acc, value_acc, query_acc)

                key_parts[number], value_parts[number], query_sum = lax.cond(
                    begin_at + block_size - 1 >= start,
                    update,
                    keep_state,
                    (key_parts[number], value_parts[number], query_sum),
                )
            return (tuple(key_parts), tuple(value_parts))

        return visitor

    zero_group = tuple(
        (jnp.zeros((count, head_count, HEAD), jnp.float32) for lower, count, start in groups)
    )

    def joined(parts):
        return parts[0].reshape(local_rows, -1)

    lse_all, terms_all = (
        lax.all_gather(lse_rows, "sp", axis=0, tiled=True),
        lax.all_gather(row_terms, "sp", axis=0, tiled=True),
    )
    plain_visit = query_side_visit(lse_all, terms_all)
    key_parts, value_parts = for_blocks(
        (zero_group, zero_group),
        (
            lax.all_gather(queries, "sp", axis=0, tiled=True),
            lax.all_gather(out_grad, "sp", axis=0, tiled=True),
        ),
        plain_visit,
    )
    (query_parts,) = for_blocks(
        (zero_group,),
        (
            lax.all_gather(keys, "sp", axis=0, tiled=True),
            lax.all_gather(values, "sp", axis=0, tiled=True),
        ),
        key_side_visit(),
    )
    query_grad = joined(query_parts)
    key_grad = joined(key_parts)
    value_grad = joined(value_parts)
    grad_rounded = query_grad.astype(jnp.bfloat16)
    input_whole = lax.all_gather(layer_input, "tp", axis=1, tiled=True)
    weight_term = lax.dot_general(
        input_whole, grad_rounded, (((0,), (0,)), ((), ())), preferred_element_type=jnp.float32
    )
    weight_grad = lax.psum_scatter(
        weight_term.astype(jnp.bfloat16), "sp", scatter_dimension=0, tiled=True
    ).astype(jnp.float32)
    return (query_grad, key_grad, value_grad, weight_grad)


def solution(mesh):
    placed = (
        P("sp", "tp"),
        P("sp", "tp"),
        P("sp", "tp"),
        P("sp", "tp"),
        P("sp", "tp"),
        P("sp", "tp"),
    )
    return jax.shard_map(
        local,
        mesh=mesh,
        in_specs=placed,
        out_specs=(P("sp", "tp"), P("sp", "tp"), P("sp", "tp"), P("sp", "tp")),
        check_vma=False,
    )
```

profile of v0, /device:TPU:0, one launch (start us, length us, event | category | flops | bytes accessed | tf_op | source)
XLA Modules:
  0.0 553.9 jit_solution(930219044404336933)
XLA Ops:
  14.1 33.1 %all_gather.27 = f32[4096,4]{0,1:T(4,128)S(1)} all-gather(f32[512,4]{0,1:T(4,128)S(1)} %bitcast.188), channel_id=1, replica_groups=mesh['sp'=8,'tp'=4] {'sp'}, dimensions={0}, use_global_device_ids=true | all-gather | bytes 73728 | tf_op jit(solution)/shard_map/all_gather | solution.py:38
  48.9 37.3 %all-gather.6.cloned.1.call-done = bf16[4096,512]{1,0:T(8,128)(2,1)} async-done(((bf16[512,512]{1,0:T(8,128)(2,1)}), bf16[4096,512]{1,0:T(8,128)(2,1)}) %all-gather.6.cloned.1.call-update) | async-done | bytes 4194320 | tf_op jit(solution)/shard_map/all_gather | solution.py:280
  86.1 6.4 %copy.117 = bf16[8,512,512]{1,2,0:T(8,128)(2,1)} copy(bf16[8,512,512]{2,1,0:T(8,128)(2,1)} %bitcast.170) | data formatting | bytes 8388608
  92.5 67.0 %all-gather.8.cloned.1.call-done = bf16[4096,512]{1,0:T(8,128)(2,1)} async-done(((bf16[512,512]{1,0:T(8,128)(2,1)}), bf16[4096,512]{1,0:T(8,128)(2,1)}) %all-gather.8.cloned.1.call-update) | async-done | bytes 4194320 | tf_op jit(solution)/shard_map/all_gather | solution.py:281
  159.6 6.4 %copy.114 = bf16[8,512,512]{1,2,0:T(8,128)(2,1)} copy(bf16[8,512,512]{2,1,0:T(8,128)(2,1)} %bitcast.171) | data formatting | bytes 8388608
  166.1 18.0 %while.51 = (s32[]{:T(128)}, f32[4,512]{1,0:T(4,128)S(1)}, f32[4,512]{1,0:T(4,128)S(1)}, f32[512,4,128]{2,0,1:T(8,128)S(1)}, s32[8]{0:T(128)S(1)}, /*index=5*/s3...) while((s32[]{:T(128)}, f32[4,512]{1,0:T(4,128)S(1)}, ...), condition=%wide.region_8.9_spmd.clone, body=%wide.region_3.8_spmd.clone.sunk | while | flops 555490304 | bytes 19609988 | solution.py:77
  167.5 6.9 %conditional.10 = ((f32[4,512]{1,0:T(4,128)S(1)}, f32[4,512]{1,0:T(4,128)S(1)}, f32[512,4,128]{2,0,1:T(8,128)S(1)})) conditional(s32[]{:T(128)} %convert_element_type.114, (f32[4,512]{1,0:T(4,128)S(1)}, f32[4,512]{1,0:T(4,128)S(1)}, f32[512,4,128]{2,0,1:T(8,128)S(1)}) %tuple.173, (s32[]{:T(128)}, s32[512]{0:T(512)S(1)}, s32[]{:T(128)}, ...), branch_computations={%region_4.4_spmd, %region_5.7_spmd} | conditional | flops 555490304 | bytes 19607634 | solution.py:115
  167.8 1.5 constant_dynamic-slice_fusion
  169.3 1.4 fusion.6
  170.8 1.4 fusion.10
  172.2 2.2 fusion.17
  184.7 19.1 %while.52 = (s32[]{:T(128)}, f32[512,4,128]{2,0,1:T(8,128)S(1)}, s32[8]{0:T(128)S(1)}, s32[]{:T(128)}, bf16[8,512,512]{1,2,0:T(8,128)(2,1)}, /*index=5*/bf16[512...) while((s32[]{:T(128)}, f32[512,4,128]{2,0,1:T(8,128)S(1)}, ...), condition=%wide.region_13.14_spmd.clone, body=%wide.region_10.13_spmd.clone.sunk | while | flops 814482432 | bytes 15792485 | solution.py:77
  185.9 9.4 %conditional.11 = (f32[512,4,128]{2,0,1:T(8,128)S(1)}) conditional(s32[]{:T(128)} %convert_element_type.115, f32[512,4,128]{2,0,1:T(8,128)S(1)} %get-tuple-element.1695, (s32[]{:T(128)}, s32[512]{0:T(512)S(1)}, s32[]{:T(128)}, bf16[8,512,512]{1,2,0:T(8,128)(2,1)}, s32[]{:T(128)}, /*index=5*/bf16[512,4,128]{2,0,1:T(8,128)(2,1)S(1)}, ...), branch_computations={%region_11.11_spmd, %region_12.12_spmd} | conditional | flops 814482432 | bytes 15790138 | solution.py:188
  185.9 1.3 constant_dynamic-slice_fusion.2
  187.2 2.8 fusion.52
  190.2 5.0 fusion.27
  204.8 1.4 copy_bitcast_fusion.2
  206.3 6.9 %fusion.48 = bf16[4096,512]{0,1:T(8,128)(2,1)} fusion(bf16[512,4096]{1,0:T(8,128)(2,1)} %all-gather.14.cloned.1.call-done, f32[512,512]{1,0:T(8,128)S(1)} %copy_bitcast_fusion.2), kind=kOutput, calls=%fused_computation.65 | convolution fusion | flops 2149842944 | bytes 9437184 | tf_op jit(solution)/shard_map/dot_general | solution.py:290
  216.0 53.0 %all-gather.10.cloned.1.call-done = bf16[4096,512]{1,0:T(8,128)(2,1)} async-done(((bf16[512,512]{1,0:T(8,128)(2,1)}), bf16[4096,512]{1,0:T(8,128)(2,1)}) %all-gather.10.cloned.1.call-update) | async-done | bytes 4194320 | tf_op jit(solution)/shard_map/all_gather | solution.py:272
  269.0 6.4 %copy.124 = bf16[8,512,512]{1,2,0:T(8,128)(2,1)} copy(bf16[8,512,512]{2,1,0:T(8,128)(2,1)} %bitcast.168) | data formatting | bytes 8388608
  275.5 66.9 %all-gather.12.cloned.1.call-done = bf16[4096,512]{1,0:T(8,128)(2,1)} async-done(((bf16[512,512]{1,0:T(8,128)(2,1)}), bf16[4096,512]{1,0:T(8,128)(2,1)}) %all-gather.12.cloned.1.call-update) | async-done | bytes 4194320 | tf_op jit(solution)/shard_map/all_gather | solution.py:273
  342.3 6.5 %copy.126 = bf16[8,512,512]{1,2,0:T(8,128)(2,1)} copy(bf16[8,512,512]{2,1,0:T(8,128)(2,1)} %bitcast.169) | data formatting | bytes 8388608
  348.9 31.7 %all_gather.30 = f32[4096,4]{0,1:T(4,128)S(1)} all-gather(f32[512,4]{0,1:T(4,128)S(1)} %bitcast.186), channel_id=1, replica_groups=mesh['sp'=8,'tp'=4] {'sp'}, dimensions={0}, use_global_device_ids=true | all-gather | bytes 73728 | tf_op jit(solution)/shard_map/all_gather | solution.py:266
  380.6 30.7 %all_gather.29 = f32[4096,4]{0,1:T(4,128)S(1)} all-gather(f32[512,4]{0,1:T(4,128)S(1)} %bitcast.187), channel_id=1, replica_groups=mesh['sp'=8,'tp'=4] {'sp'}, dimensions={0}, use_global_device_ids=true | all-gather | bytes 73728 | tf_op jit(solution)/shard_map/all_gather | solution.py:265
  412.5 129.5 %while.53 = (s32[]{:T(128)}, f32[512,4,128]{2,0,1:T(8,128)S(1)}, f32[512,4,128]{2,0,1:T(8,128)}, s32[8]{0:T(128)S(1)}, s32[]{:T(128)}, /*index=5*/f32[4096,4]{0,...) while((s32[]{:T(128)}, f32[512,4,128]{2,0,1:T(8,128)S(1)}, ...), condition=%wide.region_17.18_spmd.clone.clone, body=%wide.region_14.17_spmd.clone.clone.sunk | while | flops 1089471488 | bytes 22927804 | solution.py:77
  413.8 15.0 %conditional.12 = ((f32[512,4,128]{2,0,1:T(8,128)S(1)}, f32[512,4,128]{2,0,1:T(8,128)})) conditional(s32[]{:T(128)} %convert_element_type.116, (f32[512,4,128]{2,0,1:T(8,128)S(1)}, f32[512,4,128]{2,0,1:T(8,128)}) %tuple.179, (s32[]{:T(128)}, s32[]{:T(128)}, s32[512]{0:T(512)S(1)}, bf16[8,512,512]{1,2,0:T(8,128)(2,1)}, s32[]{:T(128)}, ...), branch_computations={%region_15.15_spmd, %region_16.16_spmd} | conditional | flops 1089471488 | bytes 22892584 | solution.py:247
  413.8 1.3 constant_dynamic-slice_fusion.4
  415.1 2.7 fusion.53
  418.1 5.3 fusion.43
  423.4 5.4 fusion.38
  430.0 14.9 %conditional.12 = ((f32[512,4,128]{2,0,1:T(8,128)S(1)}, f32[512,4,128]{2,0,1:T(8,128)})) conditional(s32[]{:T(128)} %convert_element_type.116, (f32[512,4,128]{2,0,1:T(8,128)S(1)}, f32[512,4,128]{2,0,1:T(8,128)}) %tuple.179, (s32[]{:T(128)}, s32[]{:T(128)}, s32[512]{0:T(512)S(1)}, bf16[8,512,512]{1,2,0:T(8,128)(2,1)}, s32[]{:T(128)}, ...), branch_computations={%region_15.15_spmd, %region_16.16_spmd} | conditional | flops 1089471488 | bytes 22892584 | solution.py:247
  430.1 1.3 constant_dynamic-slice_fusion.4
  431.3 2.7 fusion.53
  434.4 5.3 fusion.43
  439.6 5.3 fusion.38
  446.2 14.9 %conditional.12 = ((f32[512,4,128]{2,0,1:T(8,128)S(1)}, f32[512,4,128]{2,0,1:T(8,128)})) conditional(s32[]{:T(128)} %convert_element_type.116, (f32[512,4,128]{2,0,1:T(8,128)S(1)}, f32[512,4,128]{2,0,1:T(8,128)}) %tuple.179, (s32[]{:T(128)}, s32[]{:T(128)}, s32[512]{0:T(512)S(1)}, bf16[8,512,512]{1,2,0:T(8,128)(2,1)}, s32[]{:T(128)}, ...), branch_computations={%region_15.15_spmd, %region_16.16_spmd} | conditional | flops 1089471488 | bytes 22892584 | solution.py:247
  446.2 1.3 constant_dynamic-slice_fusion.4
  447.5 2.7 fusion.53
  450.5 5.3 fusion.43
  455.8 5.3 fusion.38
  462.4 14.9 %conditional.12 = ((f32[512,4,128]{2,0,1:T(8,128)S(1)}, f32[512,4,128]{2,0,1:T(8,128)})) conditional(s32[]{:T(128)} %convert_element_type.116, (f32[512,4,128]{2,0,1:T(8,128)S(1)}, f32[512,4,128]{2,0,1:T(8,128)}) %tuple.179, (s32[]{:T(128)}, s32[]{:T(128)}, s32[512]{0:T(512)S(1)}, bf16[8,512,512]{1,2,0:T(8,128)(2,1)}, s32[]{:T(128)}, ...), branch_computations={%region_15.15_spmd, %region_16.16_spmd} | conditional | flops 1089471488 | bytes 22892584 | solution.py:247
  462.4 1.3 constant_dynamic-slice_fusion.4
  463.7 2.7 fusion.53
  466.7 5.3 fusion.43
  472.0 5.3 fusion.38
  478.6 14.9 %conditional.12 = ((f32[512,4,128]{2,0,1:T(8,128)S(1)}, f32[512,4,128]{2,0,1:T(8,128)})) conditional(s32[]{:T(128)} %convert_element_type.116, (f32[512,4,128]{2,0,1:T(8,128)S(1)}, f32[512,4,128]{2,0,1:T(8,128)}) %tuple.179, (s32[]{:T(128)}, s32[]{:T(128)}, s32[512]{0:T(512)S(1)}, bf16[8,512,512]{1,2,0:T(8,128)(2,1)}, s32[]{:T(128)}, ...), branch_computations={%region_15.15_spmd, %region_16.16_spmd} | conditional | flops 1089471488 | bytes 22892584 | solution.py:247
  478.6 1.3 constant_dynamic-slice_fusion.4
  479.9 2.7 fusion.53
  482.9 5.3 fusion.43
  488.2 5.3 fusion.38
  494.8 14.9 %conditional.12 = ((f32[512,4,128]{2,0,1:T(8,128)S(1)}, f32[512,4,128]{2,0,1:T(8,128)})) conditional(s32[]{:T(128)} %convert_element_type.116, (f32[512,4,128]{2,0,1:T(8,128)S(1)}, f32[512,4,128]{2,0,1:T(8,128)}) %tuple.179, (s32[]{:T(128)}, s32[]{:T(128)}, s32[512]{0:T(512)S(1)}, bf16[8,512,512]{1,2,0:T(8,128)(2,1)}, s32[]{:T(128)}, ...), branch_computations={%region_15.15_spmd, %region_16.16_spmd} | conditional | flops 1089471488 | bytes 22892584 | solution.py:247
  496.0 2.7 fusion.53
  499.1 5.3 fusion.43
  504.3 5.3 fusion.38
  510.9 14.9 %conditional.12 = ((f32[512,4,128]{2,0,1:T(8,128)S(1)}, f32[512,4,128]{2,0,1:T(8,128)})) conditional(s32[]{:T(128)} %convert_element_type.116, (f32[512,4,128]{2,0,1:T(8,128)S(1)}, f32[512,4,128]{2,0,1:T(8,128)}) %tuple.179, (s32[]{:T(128)}, s32[]{:T(128)}, s32[512]{0:T(512)S(1)}, bf16[8,512,512]{1,2,0:T(8,128)(2,1)}, s32[]{:T(128)}, ...), branch_computations={%region_15.15_spmd, %region_16.16_spmd} | conditional | flops 1089471488 | bytes 22892584 | solution.py:247
  512.2 2.7 fusion.53
  515.2 5.3 fusion.43
  520.5 5.3 fusion.38
  527.1 14.9 %conditional.12 = ((f32[512,4,128]{2,0,1:T(8,128)S(1)}, f32[512,4,128]{2,0,1:T(8,128)})) conditional(s32[]{:T(128)} %convert_element_type.116, (f32[512,4,128]{2,0,1:T(8,128)S(1)}, f32[512,4,128]{2,0,1:T(8,128)}) %tuple.179, (s32[]{:T(128)}, s32[]{:T(128)}, s32[512]{0:T(512)S(1)}, bf16[8,512,512]{1,2,0:T(8,128)(2,1)}, s32[]{:T(128)}, ...), branch_computations={%region_15.15_spmd, %region_16.16_spmd} | conditional | flops 1089471488 | bytes 22892584 | solution.py:247
  528.4 2.7 fusion.53
  531.4 5.3 fusion.43
  536.7 5.3 fusion.38
  542.0 2.8 copy_bitcast_fusion
  544.8 2.2 copy.130
  (168 shorter events, 35.7 us)
Async XLA Ops:
  7.2 4.7 copy-start.4
  7.2 5.2 copy-start.5
  7.2 78.9 %all-gather.6.cloned.1.call-start = ((), (), s32[]{:S(2)}) async-start(), calls=%async_computation.1 | async-start | bytes 4718592 | tf_op jit(solution)/shard_map/all_gather | solution.py:280
  7.9 151.7 %all-gather.8.cloned.1.call-start = ((), (), s32[]{:S(2)}) async-start(), calls=%async_computation.2 | async-start | bytes 4718592 | tf_op jit(solution)/shard_map/all_gather | solution.py:281
  8.7 197.6 %all-gather.14.cloned.1.call-start = ((), (), s32[]{:S(2)}) async-start(), calls=%async_computation.5 | async-start | bytes 5242880 | tf_op jit(solution)/shard_map/all_gather | solution.py:289
  9.4 259.6 %all-gather.10.cloned.1.call-start = ((), (), s32[]{:S(2)}) async-start(), calls=%async_computation.3 | async-start | bytes 4718592 | tf_op jit(solution)/shard_map/all_gather | solution.py:272
  10.0 332.4 %all-gather.12.cloned.1.call-start = ((), (), s32[]{:S(2)}) async-start(), calls=%async_computation.4 | async-start | bytes 4718592 | tf_op jit(solution)/shard_map/all_gather | solution.py:273
  10.6 534.3 %reduce-scatter.2.cloned.1.call-start = ((), (), s32[]{:S(2)}) async-start(), calls=%async_computation.6 | async-start | bytes 4718592 | tf_op jit(solution)/shard_map/reduce_scatter | solution.py:293
  203.9 1.0 copy-start.1
  206.3 6.9 %copy-start = (f32[512,512]{1,0:T(8,128)}, f32[512,512]{1,0:T(8,128)S(1)}, u32[]{:S(2)}) copy-start(f32[512,512]{1,0:T(8,128)S(1)} %copy_bitcast_fusion.2) | copy-start | bytes 3145732
  213.2 1.0 copy-start.2
  213.2 1.3 copy-start.3
Sparse Core Ops, SparseCore 0:
  10.1 75.9 all-gather.5
  88.2 71.3 all-gather.7
  161.1 32.9 all-gather.13
  196.2 72.8 all-gather.9
  271.0 71.3 all-gather.11
  345.8 88.3 reduce-scatter.1
where the time goes:
time: 556 us; the launch traced here: 554 us
  waiting for transfers between devices  227 us (41%)
  matrix products  125 us (22%)
  blocking collectives  95.6 us (17%)
  local copies, waits for them, and re-layouts  69.6 us (13%)
  loops' own time  16.7 us (3%)
  between operations  14.3 us (3%)
    all_gather x1, waiting for transfers between devices, local(): lax.all_gather(values, 'sp', axis=0, tiled=True)  67 us
    all_gather x1, waiting for transfers between devices, local(): lax.all_gather(out_grad, 'sp', axis=0, tiled=True)  66.9 us
    all_gather x1, waiting for transfers between devices, local(): lax.all_gather(queries, 'sp', axis=0, tiled=True)  53 us
    dot_general x8, matrix products, update(): jnp.einsum('hqk,qhd->khd', prob_rows.astype(jnp.bfloat16), block_grads, p...  42.5 us
    dot_general x8, matrix products, update(): jnp.einsum('hqk,qhd->khd', score_grad, block_queries, preferred_element_t...  42.2 us
    all_gather x1, waiting for transfers between devices, local(): lax.all_gather(keys, 'sp', axis=0, tiled=True)  37.3 us
    unnamed x30, local copies, waits for them, and re-layouts  34.8 us
    all_gather x1, blocking collectives, local(): gathered_gates = lax.all_gather(local_gates, 'sp', axis=0, tiled=True)  33.1 us
  transfers between devices with their start and end apart: 6, of which 4 were waited for; matrix products, arithmetic and copies ran while one was open for 35% of the time, Pallas kernels for 0%

commit v1 on v0

v1 whole, which is shorter than its diff:
```python
import jax
import jax.numpy as jnp
from jax import lax
from jax.experimental import pallas as pl
from jax.experimental.pallas import tpu as pltpu
from jax.sharding import PartitionSpec as P

HEAD = 128
LOG2E = 1.4426950408889634
SCALE = HEAD ** (-0.5)


def nt(a, b):
    return lax.dot_general(a, b, (((1,), (1,)), ((), ())), preferred_element_type=jnp.float32)


def nn(a, b):
    return lax.dot_general(a, b, (((1,), (0,)), ((), ())), preferred_element_type=jnp.float32)


def attention_kernel(parts, q_ref, g_ref, k_ref, v_ref, gate_ref, dq_ref, dk_ref, dv_ref, kt, vt, sc, dk, dv):
    blocks, rows, _ = k_ref.shape
    sub = q_ref.shape[1]
    part = lax.rem(lax.axis_index("sp"), parts)

    @pl.loop(0, blocks)
    def _(j):
        kt[j] = k_ref[j].T
        vt[j] = v_ref[j].T
        dk[j] = jnp.zeros((rows, HEAD), jnp.float32)
        dv[j] = jnp.zeros((rows, HEAD), jnp.float32)

    @pl.loop(0, blocks)
    def _(b):
        q = q_ref[b]
        g = g_ref[b]
        offset = lax.rem(part + b, parts) * sub

        def score(j):
            return nt(k_ref[j], q) * (SCALE * LOG2E) - gate_ref[j]

        def pass_a(j, top):
            s = score(j)
            sc[j] = s
            return jnp.maximum(top, jnp.max(s, axis=0, keepdims=True))

        top = lax.fori_loop(0, b, pass_a, jnp.full((1, sub), -1e30, jnp.float32))
        key_pos = lax.broadcasted_iota(jnp.int32, (rows, sub), 0)
        query_pos = lax.broadcasted_iota(jnp.int32, (rows, sub), 1) + offset
        s = jnp.where(key_pos <= query_pos, score(b), -1e30)
        sc[b] = s
        top = jnp.maximum(top, jnp.max(s, axis=0, keepdims=True))

        def pass_b(j, state):
            total, mixed = state
            w = jnp.exp2(sc[j] - top)
            sc[j] = w
            total = total + jnp.sum(w, axis=0, keepdims=True)
            return total, mixed + nn(vt[j], w.astype(jnp.bfloat16))

        total, mixed = lax.fori_loop(
            0, b + 1, pass_b, (jnp.zeros((1, sub), jnp.float32), jnp.zeros((HEAD, sub), jnp.float32))
        )
        attended = (mixed / total).astype(jnp.bfloat16).astype(jnp.float32)
        terms = jnp.sum(attended * g.astype(jnp.float32).T, axis=0, keepdims=True)
        inverse = 1.0 / total

        def pass_c(j, acc):
            prob = sc[j] * inverse
            ds = (prob * (nt(v_ref[j], g) - terms)).astype(jnp.bfloat16)
            dv[j] += nn(prob.astype(jnp.bfloat16), g)
            dk[j] += nn(ds, q)
            return acc + nn(kt[j], ds)

        acc = lax.fori_loop(0, b + 1, pass_c, jnp.zeros((HEAD, sub), jnp.float32))
        dq_ref[b] = (acc * SCALE).T.astype(jnp.bfloat16)

    @pl.loop(0, blocks)
    def _(j):
        dk_ref[j] = (dk[j] * SCALE).astype(jnp.bfloat16)
        dv_ref[j] = dv[j].astype(jnp.bfloat16)


def attention(parts, q, g, k, v, gate):
    blocks, rows, _ = k.shape
    sub = q.shape[1]
    vmem = pl.BlockSpec(memory_space=pltpu.VMEM)
    low = jnp.bfloat16
    return pl.pallas_call(
        lambda *refs: attention_kernel(parts, *refs),
        out_shape=(
            jax.ShapeDtypeStruct((blocks, sub, HEAD), low),
            jax.ShapeDtypeStruct((blocks, rows, HEAD), low),
            jax.ShapeDtypeStruct((blocks, rows, HEAD), low),
        ),
        in_specs=[vmem] * 5,
        out_specs=(vmem,) * 3,
        scratch_shapes=[
            pltpu.VMEM((blocks, HEAD, rows), low),
            pltpu.VMEM((blocks, HEAD, rows), low),
            pltpu.VMEM((blocks, rows, sub), jnp.float32),
            pltpu.VMEM((blocks, rows, HEAD), jnp.float32),
            pltpu.VMEM((blocks, rows, HEAD), jnp.float32),
        ],
        compiler_params=pltpu.CompilerParams(vmem_limit_bytes=60 * 1024 * 1024),
        cost_estimate=pl.CostEstimate(
            flops=6 * blocks * blocks * rows * sub * HEAD, bytes_accessed=1 << 22, transcendentals=0
        ),
        name="attention",
    )(q, g, k, v, gate)


def local(queries, keys, values, forget_logits, layer_input, out_grad):
    rows = queries.shape[0]
    heads = queries.shape[1] // HEAD
    shards = lax.axis_size("sp")
    parts = shards // heads
    sub = rows // parts
    me = lax.axis_index("sp")
    head = me // parts
    part = me % parts

    input_whole = lax.all_gather(layer_input, "tp", axis=1, tiled=True)

    local_gates = jnp.cumsum(jax.nn.log_sigmoid(forget_logits), axis=0)
    per_shard = lax.all_gather(local_gates, "sp", axis=0)
    totals = per_shard[:, -1, :]
    before = jnp.cumsum(totals, axis=0) - totals
    sums = per_shard + before[:, None, :]
    gate = lax.dynamic_slice_in_dim(sums, head, 1, 2) * LOG2E

    def whole(a):
        a = a.reshape(rows, heads, HEAD).transpose(1, 0, 2)
        return jnp.broadcast_to(a[:, None], (heads, parts, rows, HEAD)).reshape(shards, rows, HEAD)

    def split(a):
        a = a.reshape(parts, sub, heads, HEAD).transpose(2, 0, 1, 3)
        twice = jnp.concatenate([a, a], axis=1)
        return lax.dynamic_slice_in_dim(twice, me % parts, parts, 1).reshape(shards, sub, HEAD)

    packed = jnp.concatenate([whole(keys), whole(values), split(queries), split(out_grad)], axis=1)
    got = lax.all_to_all(packed, "sp", 0, 0)
    k, v = got[:, :rows], got[:, rows : 2 * rows]
    q, g = got[:, 2 * rows : 2 * rows + sub], got[:, 2 * rows + sub :]
    dq, dk, dv = attention(parts, q, g, k, v, gate)

    back = lax.all_to_all(dq, "sp", 0, 0).reshape(heads, parts, sub, HEAD)
    twice = jnp.concatenate([back, back], axis=1)
    back = lax.dynamic_slice_in_dim(twice, parts - me % parts, parts, 1)
    low = back.transpose(1, 2, 0, 3).reshape(rows, heads * HEAD)
    weight_term = lax.dot_general(
        input_whole, low, (((0,), (0,)), ((), ())), preferred_element_type=jnp.float32
    )
    weight_grad = lax.psum_scatter(
        weight_term.astype(jnp.bfloat16), "sp", scatter_dimension=0, tiled=True
    ).astype(jnp.float32)
    both = lax.all_to_all(jnp.concatenate([dk, dv], axis=1), "sp", 0, 0)
    both = both.reshape(heads, parts, 2, rows, HEAD).astype(jnp.float32).sum(axis=1)
    both = both.transpose(1, 2, 0, 3).reshape(2, rows, heads * HEAD)
    return low.astype(jnp.float32), both[0], both[1], weight_grad


def solution(mesh):
    spec = P("sp", "tp")
    return jax.shard_map(
        local, mesh=mesh, in_specs=(spec,) * 6, out_specs=(spec,) * 4, check_vma=False
    )
```

time: 556 us -> 332 us (0.60)
  matrix products: 125 us -> 6.53 us
  waiting for transfers between devices: 227 us -> 131 us
  local copies, waits for them, and re-layouts: 69.6 us -> 13.7 us
  Pallas kernels: 0 us -> 41 us
  loops' own time: 16.7 us -> 0 us
  starting transfers between devices: 0.23 us -> 15.7 us
    all_gather x4 -> x0, waiting for transfers between devices: 224 us -> none  [the longest x1 67 us: local(): lax.all_gather(values, 'sp', axis=0, tiled=True)]
    dot_general x29 -> x1, matrix products: 125 us -> 6.53 us  [local(): lax.dot_general(input_whole, low, (((0,), (0,)), ((), ())), preferred_ele...]
    all_to_all x0 -> x3, waiting for transfers between devices: none -> 94.6 us  [the longest x1 80.2 us: local(): both = lax.all_to_all(jnp.concatenate([dk, dv], axis=1), 'sp', 0, 0)]
    pallas_call x0 -> x1, Pallas kernels: none -> 41 us  [attention(): pl.pallas_call(lambda *refs: attention_kernel(parts, *refs), out_shape=(j...]
    reduce_scatter x1, waiting for transfers between devices: 0.01 us -> 35.5 us  [local(): lax.psum_scatter(weight_term.astype(jnp.bfloat16), 'sp', scatter_dimensio...]
    unnamed x30 -> x13, local copies, waits for them, and re-layouts: 34.8 us -> 6.36 us
    dynamic_slice x35 -> x1, local copies, waits for them, and re-layouts: 27.7 us -> 0.08 us  [local(): gate = lax.dynamic_slice_in_dim(sums, head, 1, 2) * LOG2E]
    another operation x27 -> x0, loops' own time: 16.7 us -> none  [the longest x3 16.1 us: for_blocks(): current, _ = lax.scan(one_block, current, (numbers, stacked))]
  transfers between devices with their start and end apart: 6 -> 5, of which waited for: 4 -> 3; matrix products, arithmetic and copies ran while one was open for 35% -> 4% of each run, Pallas kernels for 0% -> 12%
where the time goes in v1:
time: 332 us; the launch traced here: 331 us
  waiting for transfers between devices  131 us (39%)
  blocking collectives  100 us (30%)
  Pallas kernels  41 us (12%)
  starting transfers between devices  15.7 us (5%)
  between operations  14.3 us (4%)
  local copies, waits for them, and re-layouts  13.7 us (4%)
  other arithmetic  8.81 us (3%)
  matrix products  6.53 us (2%)
    all_gather x1, blocking collectives, local(): per_shard = lax.all_gather(local_gates, 'sp', axis=0)  100 us
    all_to_all x1, waiting for transfers between devices, local(): both = lax.all_to_all(jnp.concatenate([dk, dv], axis=1), 'sp', 0, 0)  80.2 us
    pallas_call x1, Pallas kernels, attention(): pl.pallas_call(lambda *refs: attention_kernel(parts, *refs), out_shape=(j...  41 us
    reduce_scatter x1, waiting for transfers between devices, local(): lax.psum_scatter(weight_term.astype(jnp.bfloat16), 'sp', scatter_dimensio...  35.5 us
    all_to_all x1, waiting for transfers between devices, local(): back = lax.all_to_all(dq, 'sp', 0, 0).reshape(heads, parts, sub, HEAD)  14.4 us
    all_to_all x1, starting transfers between devices, local(): got = lax.all_to_all(packed, 'sp', 0, 0)  7.41 us
  transfers between devices with their start and end apart: 5, of which 3 were waited for; matrix products, arithmetic and copies ran while one was open for 4% of the time, Pallas kernels for 12%

profile of v1, /device:TPU:0, one launch (start us, length us, event | category | flops | bytes accessed | tf_op | source)
XLA Modules:
  0.0 331.3 jit_solution(6454214420596171785)
XLA Ops:
  7.2 0.0 copy-start.2
  7.2 0.0 copy-start.3
  7.2 1.2 reshape.67
  8.5 0.1 copy.60
  8.5 1.2 reshape.65
  9.7 0.1 copy.61
  9.8 0.0 copy-done.2
  9.8 0.1 reshape.61
  9.9 0.1 copy.37
  10.0 0.0 copy-done.3
  10.0 0.1 reshape.63
  10.1 0.1 copy.38
  10.2 0.4 fusion.4
  10.6 0.1 broadcast_in_dim.4
  10.8 0.1 broadcast_in_dim.5
  10.9 1.8 pad_maximum_fusion
  12.7 0.0 copy-start.4
  12.7 7.4 %all-to-all-start = ((bf16[8,1536,128]{2,1,0:T(8,128)(2,1)}), bf16[8,1536,128]{2,1,0:T(8,128)(2,1)S(1)}, u32[]{:S(2)}, u32[]{:S(2)}) async-start(bf16[8,1536,128]{2,1,0:T(8,128)(2,1)} %pad_maximum_fusion), calls=%async_computation | async-start | bytes 6291456 | tf_op jit(solution)/shard_map/all_to_all | solution.py:142
  20.1 0.0 all-gather.3.cloned.1.call-start
  20.2 0.7 all-gather.3.cloned.1.call-update
  20.9 0.0 copy-done.4
  20.9 1.2 reduce-window.6
  22.2 0.2 slice_reduce_fusion
  22.3 0.2 reduce-window.9
  22.5 0.1 broadcast_add_fusion
  22.6 0.2 copy.50
  22.8 100.4 %all-gather = f32[4096,4]{1,0:T(8,128)S(1)} all-gather(f32[512,4]{1,0:T(8,128)S(1)} %bitcast.54), channel_id=2, replica_groups=mesh['sp'=8,'tp'=4] {'sp'}, dimensions={0}, use_global_device_ids=true | all-gather | bytes 73728 | tf_op jit(solution)/shard_map/all_gather | solution.py:126
  123.2 0.1 constant_dynamic-slice_fusion
  123.3 2.0 fusion.1.refs_4_
  125.3 0.0 all-to-all-done
  125.3 1.1 fusion.12
  126.3 1.5 fusion.11
  127.8 41.0 %attention.1 = (bf16[8,256,128]{2,1,0:T(8,128)(2,1)}, bf16[8,512,128]{2,1,0:T(8,128)(2,1)}, bf16[8,512,128]{2,1,0:T(8,128)(2,1)}) custom-call(bf16[8,256,128]{2,1,0:T(8,128)(2,1)} %get-tuple-element.29.refs_0_, bf16[8,256,128]{2,1,0:T(8,128)(2,1)} %get-tuple-element.28.refs_1_, bf16[8,512,128]{2,1,0:T(8,128)(2,1)} %get-tuple-element.27.refs_2_, ...), custom_call_target="tpu_custom_call" | custom-call | flops 6442450944 | bytes 4194304 | tf_op jit(solution)/shard_map/attention/pallas_call | solution.py:89
  168.8 4.6 %all-to-all-start.1 = ((bf16[8,256,128]{2,1,0:T(8,128)(2,1)}), bf16[8,256,128]{2,1,0:T(8,128)(2,1)S(1)}, u32[]{:S(2)}, u32[]{:S(2)}) async-start(bf16[8,256,128]{2,1,0:T(8,128)(2,1)} %get-tuple-element.7), calls=%async_computation.1 | async-start | bytes 1048576 | tf_op jit(solution)/shard_map/all_to_all | solution.py:147
  173.4 0.0 reduce-scatter.2.cloned.1.call-start
  173.4 14.4 %all-to-all-done.1 = bf16[8,256,128]{2,1,0:T(8,128)(2,1)S(1)} async-done(((bf16[8,256,128]{2,1,0:T(8,128)(2,1)}), bf16[8,256,128]{2,1,0:T(8,128)(2,1)S(1)}, u32[]{:S(2)}, u32[]{:S(2)}) %all-to-all-start.1) | async-done | bytes 524320 | tf_op jit(solution)/shard_map/all_to_all | solution.py:147
  187.8 0.2 fusion.3
  188.0 0.4 copy.44
  188.4 0.0 all-gather.3.cloned.1.call-done
  188.5 6.5 %fusion = bf16[4096,512]{0,1:T(8,128)(2,1)} fusion(bf16[512,4096]{1,0:T(8,128)(2,1)} %all-gather.3.cloned.1.call-done, bf16[64,8,4,128]{3,2,1,0:T(4,128)(2,1)S(1)} %bitcast.41), kind=kOutput, calls=%fused_computation.1 | convolution fusion | flops 2149580800 | bytes 8912896 | tf_op jit(solution)/shard_map/dot_general | solution.py:151
  195.0 0.0 copy-start
  195.0 0.0 copy-start.1
  195.0 0.0 reduce-scatter.2.cloned.1.call-update
  195.0 1.2 copy-done
  196.2 0.3 copy-done.1
  196.5 1.5 pad_maximum_fusion.1
  198.0 3.6 %all-to-all-start.2 = ((bf16[8,1024,128]{2,1,0:T(8,128)(2,1)}), bf16[8,1024,128]{2,1,0:T(8,128)(2,1)S(1)}, u32[]{:S(2)}, u32[]{:S(2)}) async-start(bf16[8,1024,128]{2,1,0:T(8,128)(2,1)} %pad_maximum_fusion.1), calls=%async_computation.2 | async-start | bytes 4194304 | tf_op jit(solution)/shard_map/all_to_all | solution.py:157
  201.6 1.1 bitcast_convert_fusion
  202.7 80.2 %all-to-all-done.2 = bf16[8,1024,128]{2,1,0:T(8,128)(2,1)S(1)} async-done(((bf16[8,1024,128]{2,1,0:T(8,128)(2,1)}), bf16[8,1024,128]{2,1,0:T(8,128)(2,1)S(1)}, u32[]{:S(2)}, u32[]{:S(2)}) %all-to-all-start.2) | async-done | bytes 2097184 | tf_op jit(solution)/shard_map/all_to_all | solution.py:157
  283.0 0.3 convert_reduce_fusion
  283.3 0.1 fusion.13
  283.5 0.3 copy.45
  283.8 1.3 copy.47
  285.1 0.3 copy.46
  285.5 1.3 copy.48
  286.8 35.5 %reduce-scatter.2.cloned.1.call-done = bf16[512,512]{0,1:T(8,128)(2,1)} async-done(((bf16[4096,512]{0,1:T(8,128)(2,1)}), bf16[512,512]{0,1:T(8,128)(2,1)}) %reduce-scatter.2.cloned.1.call-update) | async-done | bytes 524304 | tf_op jit(solution)/shard_map/reduce_scatter | solution.py:154
  322.3 2.2 copy.49
  (3 shorter events, 0.0 us)
Async XLA Ops:
  7.2 2.6 copy-start.2
  7.2 2.8 copy-start.3
  12.7 8.2 %copy-start.4 = (f32[512,4]{0,1:T(4,128)S(1)}, f32[512,4]{0,1:T(4,128)}, u32[]{:S(2)}) copy-start(f32[512,4]{0,1:T(4,128)} %param.9) | copy-start | bytes 24580
  12.7 112.5 %all-to-all-start = ((bf16[8,1536,128]{2,1,0:T(8,128)(2,1)}), bf16[8,1536,128]{2,1,0:T(8,128)(2,1)S(1)}, u32[]{:S(2)}, u32[]{:S(2)}) async-start(bf16[8,1536,128]{2,1,0:T(8,128)(2,1)} %pad_maximum_fusion), calls=%async_computation | async-start | bytes 6291456 | tf_op jit(solution)/shard_map/all_to_all | solution.py:142
  20.1 168.3 %all-gather.3.cloned.1.call-start = ((), (), s32[]{:S(2)}) async-start(), calls=%async_computation.4 | async-start | bytes 5242880 | tf_op jit(solution)/shard_map/all_gather | solution.py:123
  168.8 19.0 %all-to-all-start.1 = ((bf16[8,256,128]{2,1,0:T(8,128)(2,1)}), bf16[8,256,128]{2,1,0:T(8,128)(2,1)S(1)}, u32[]{:S(2)}, u32[]{:S(2)}) async-start(bf16[8,256,128]{2,1,0:T(8,128)(2,1)} %get-tuple-element.7), calls=%async_computation.1 | async-start | bytes 1048576 | tf_op jit(solution)/shard_map/all_to_all | solution.py:147
  173.4 148.9 %reduce-scatter.2.cloned.1.call-start = ((), (), s32[]{:S(2)}) async-start(), calls=%async_computation.5 | async-start | bytes 4718592 | tf_op jit(solution)/shard_map/reduce_scatter | solution.py:154
  195.0 1.2 copy-start
  195.0 1.5 copy-start.1
  198.0 85.0 %all-to-all-start.2 = ((bf16[8,1024,128]{2,1,0:T(8,128)(2,1)}), bf16[8,1024,128]{2,1,0:T(8,128)(2,1)S(1)}, u32[]{:S(2)}, u32[]{:S(2)}) async-start(bf16[8,1024,128]{2,1,0:T(8,128)(2,1)} %pad_maximum_fusion.1), calls=%async_computation.2 | async-start | bytes 4194304 | tf_op jit(solution)/shard_map/all_to_all | solution.py:157
Sparse Core Ops, SparseCore 0:
  22.5 35.8 all-gather.2
  195.1 127.0 reduce-scatter.1

commit v2 on v1

v2 whole, which is shorter than its diff:
```python
import jax
import jax.numpy as jnp
from jax import lax
from jax.experimental import pallas as pl
from jax.experimental.pallas import tpu as pltpu
from jax.sharding import PartitionSpec as P

HEAD = 128
LOG2E = 1.4426950408889634
SCALE = HEAD ** (-0.5)
LOW = jnp.bfloat16


def nt(a, b):
    return lax.dot_general(a, b, (((1,), (1,)), ((), ())), preferred_element_type=jnp.float32)


def nn(a, b):
    return lax.dot_general(a, b, (((1,), (0,)), ((), ())), preferred_element_type=jnp.float32)


def kernel_body(
    heads, parts,
    q_in, g_in, k_in, v_in, gate_in,
    dq_out, low_out, dk_out, dv_out,
    kv, qg, gates, kt, vt, bias, sc, dk, dv, dq_stage, part_stage, red, fin, dq_got, kv_got,
    kv_recv, qg_recv, gate_recv, kv_send, qg_send, gate_send, relay_send,
    dq_send, dq_recv, part_send, red_recv, fin_send, fin_recv, local_sem,
):
    blocks, _, rows, _ = kv.shape
    sub = qg.shape[2]
    per_part = blocks // parts
    me = lax.axis_index("sp")
    head = me // parts
    part = lax.rem(me, parts)

    def remote(src, dst, send, recv, target):
        return pltpu.make_async_remote_copy(
            src_ref=src, dst_ref=dst, send_sem=send, recv_sem=recv, device_id={"sp": target}
        )

    barrier = pltpu.get_barrier_semaphore()
    for r in range(1, blocks):
        pl.semaphore_signal(barrier, inc=1, device_id={"sp": lax.rem(me + r, blocks)})
    pl.semaphore_wait(barrier, blocks - 1)

    def lanes(h):
        return pl.ds(pl.multiple_of(h * HEAD, HEAD), HEAD)

    sources = ((k_in, v_in), (q_in, g_in))

    def place(r, c):
        return lax.rem(head + r, heads), lax.rem(part + c, parts)

    def kv_copy(r, i):
        h, _ = place(r, 0)
        return remote(
            sources[0][i].at[:, lanes(h)], kv.at[me, i], kv_send.at[r, i], kv_recv.at[me, i], h * parts + part
        )

    def relay_copy(r, c, i):
        h, other = place(r, c)
        j = h * parts + part
        src = sources[0][i].at[:, lanes(head)] if r == 0 else kv.at[j, i]
        return remote(src, kv.at[j, i], relay_send.at[r, c, i], kv_recv.at[j, i], head * parts + other)

    def q_source(r, c, i):
        h, other = place(r, c)
        begin = pl.multiple_of(lax.rem(other + me, parts) * sub, sub)
        return sources[1][i].at[pl.ds(begin, sub), lanes(h)]

    def q_copy(r, c, i):
        h, other = place(r, c)
        return remote(
            q_source(r, c, i), qg.at[me, i], qg_send.at[r, c, i], qg_recv.at[me, i], h * parts + other
        )

    def gate_copy(r, c):
        h, other = place(r, c)
        return remote(gate_in.at[h], gates.at[me], gate_send.at[r, c], gate_recv.at[me], h * parts + other)

    pairs = [(r, c) for r in range(heads) for c in range(parts) if (r, c) != (0, 0)]
    for r in range(1, heads):
        for i in range(2):
            kv_copy(r, i).start()
    for c in range(1, parts):
        for i in range(2):
            relay_copy(0, c, i).start()
    for r, c in pairs:
        gate_copy(r, c).start()
        for i in range(2):
            q_copy(r, c, i).start()
    own = [
        pltpu.make_async_copy(sources[0][i].at[:, lanes(head)], kv.at[me, i], local_sem.at[i]) for i in range(2)
    ]
    own += [pltpu.make_async_copy(q_source(0, 0, i), qg.at[me, i], local_sem.at[2 + i]) for i in range(2)]
    own += [pltpu.make_async_copy(gate_in.at[head], gates.at[me], local_sem.at[4])]
    for copy in own:
        copy.start()

    def kv_wait(j):
        for i in range(2):
            remote(kv.at[j, i], kv.at[j, i], kv_send.at[0, i], kv_recv.at[j, i], me).wait_recv()

    for r in range(1, heads):
        j = place(r, 0)[0] * parts + part
        kv_wait(j)
        for c in range(1, parts):
            for i in range(2):
                relay_copy(r, c, i).start()
    for copy in own:
        copy.wait()
    for r, c in pairs:
        h, other = place(r, c)
        j = h * parts + other
        if c:
            kv_wait(j)
        for i in range(2):
            remote(qg.at[j, i], qg.at[j, i], qg_send.at[0, 0, i], qg_recv.at[j, i], me).wait_recv()
        remote(gates.at[j], gates.at[j], gate_send.at[0, 0], gate_recv.at[j], me).wait_recv()

    def prepare(j, base):
        kt[j] = kv[j, 0].T
        vt[j] = kv[j, 1].T
        row = gates[j, 0:1] + base
        bias[j] = jnp.broadcast_to(row, (HEAD, rows)).T
        dk[j] = jnp.zeros((rows, HEAD), jnp.float32)
        dv[j] = jnp.zeros((rows, HEAD), jnp.float32)
        return base + gates[j, 1:2]

    lax.fori_loop(0, blocks, prepare, jnp.zeros((1, rows), jnp.float32))

    def compute(b):
        q = qg[b, 0]
        g = qg[b, 1]
        offset = lax.rem(part + b, parts) * sub

        def score(j):
            return nt(kv[j, 0], q) * (SCALE * LOG2E) - bias[j][:, 0:1]

        def pass_a(j, top):
            s = score(j)
            sc[j] = s
            return jnp.maximum(top, jnp.max(s, axis=0, keepdims=True))

        top = lax.fori_loop(0, b, pass_a, jnp.full((1, sub), -1e30, jnp.float32))
        key_pos = lax.broadcasted_iota(jnp.int32, (rows, sub), 0)
        query_pos = lax.broadcasted_iota(jnp.int32, (rows, sub), 1) + offset
        s = jnp.where(key_pos <= query_pos, score(b), -1e30)
        sc[b] = s
        top = jnp.maximum(top, jnp.max(s, axis=0, keepdims=True))

        def pass_b(j, state):
            total, mixed = state
            w = jnp.exp2(sc[j] - top)
            sc[j] = w
            total = total + jnp.sum(w, axis=0, keepdims=True)
            return total, mixed + nn(vt[j], w.astype(LOW))

        total, mixed = lax.fori_loop(
            0, b + 1, pass_b, (jnp.zeros((1, sub), jnp.float32), jnp.zeros((HEAD, sub), jnp.float32))
        )
        attended = (mixed / total).astype(LOW).astype(jnp.float32)
        terms = jnp.sum(attended * g.astype(jnp.float32).T, axis=0, keepdims=True)
        inverse = 1.0 / total

        def pass_c(j, acc):
            prob = sc[j] * inverse
            ds = (prob * (nt(kv[j, 1], g) - terms)).astype(LOW)
            dv[j] += nn(prob.astype(LOW), g)
            dk[j] += nn(ds, q)
            return acc + nn(kt[j], ds)

        acc = lax.fori_loop(0, b + 1, pass_c, jnp.zeros((HEAD, sub), jnp.float32))
        dq_stage[b] = (acc * SCALE).T.astype(LOW)
        part_stage[b, 0] = (dk[b] * SCALE).astype(LOW)
        part_stage[b, 1] = dv[b].astype(LOW)

    def dq_copy(b):
        return remote(
            dq_stage.at[b], dq_got.at[head, lax.rem(part + b, parts)], dq_send.at[b], dq_recv.at[me], b
        )

    def part_copy(b):
        return remote(
            part_stage.at[b],
            red.at[b // parts, part],
            part_send.at[b],
            red_recv.at[b // parts, part],
            head * parts + lax.rem(b, parts),
        )

    def fin_copy(b):
        return remote(fin.at[b // parts], kv_got.at[head], fin_send.at[b // parts], fin_recv.at[head], b)

    def step(s, carry):
        b = blocks - 1 - s

        @pl.when(s < blocks)
        def _():
            compute(b)

        @pl.when((s >= 1) & (s < blocks + 1))
        def _():
            n = b + 1

            @pl.when(n == me)
            def _():
                dq_got[head, lax.rem(part + n, parts)] = dq_stage[n]

            @pl.when(n != me)
            def _():
                dq_copy(n).start()

            @pl.when(lax.rem(n, parts) != part)
            def _():
                part_copy(n).start()

        @pl.when((s >= 2) & (s < blocks + 2))
        def _():
            n = b + 2

            @pl.when(lax.rem(n, parts) == part)
            def _():
                slot = n // parts
                for c in range(1, parts):
                    other = lax.rem(part + c, parts)
                    remote(
                        red.at[slot, other], red.at[slot, other], part_send.at[0], red_recv.at[slot, other], me
                    ).wait_recv()
                for i in range(2):
                    value = dk[n] * SCALE if i == 0 else dv[n]
                    for c in range(1, parts):
                        value = value + red[slot, lax.rem(part + c, parts), i].astype(jnp.float32)
                    fin[slot, i] = value.astype(LOW)

        @pl.when(s >= 3)
        def _():
            n = b + 3

            @pl.when(lax.rem(n, parts) == part)
            def _():
                @pl.when(n == me)
                def _():
                    kv_got[head] = fin[n // parts]

                @pl.when(n != me)
                def _():
                    fin_copy(n).start()

        return carry

    lax.fori_loop(0, blocks + 3, step, 0)

    for r, c in pairs:
        h, other = place(r, c)
        slot = lax.rem(other + me, parts)
        remote(
            dq_got.at[h, slot], dq_got.at[h, slot], dq_send.at[0], dq_recv.at[h * parts + other], me
        ).wait_recv()
    for h in range(heads):
        for n in range(parts):
            piece = dq_got[h, n]
            low_out[n * sub : (n + 1) * sub, h * HEAD : (h + 1) * HEAD] = piece
            dq_out[n * sub : (n + 1) * sub, h * HEAD : (h + 1) * HEAD] = piece.astype(jnp.float32)
    for r in range(1, heads):
        h, _ = place(r, 0)
        remote(kv_got.at[h], kv_got.at[h], fin_send.at[0], fin_recv.at[h], me).wait_recv()
    for h in range(heads):
        dk_out[:, h * HEAD : (h + 1) * HEAD] = kv_got[h, 0].astype(jnp.float32)
        dv_out[:, h * HEAD : (h + 1) * HEAD] = kv_got[h, 1].astype(jnp.float32)

    for r in range(1, heads):
        for i in range(2):
            kv_copy(r, i).wait_send()
    for r in range(heads):
        for c in range(1, parts):
            for i in range(2):
                relay_copy(r, c, i).wait_send()
    for r, c in pairs:
        gate_copy(r, c).wait_send()
        for i in range(2):
            q_copy(r, c, i).wait_send()

    @pl.loop(0, blocks)
    def _(b):
        @pl.when(b != me)
        def _():
            dq_copy(b).wait_send()

        @pl.when(lax.rem(b, parts) != part)
        def _():
            part_copy(b).wait_send()

        @pl.when((lax.rem(b, parts) == part) & (b != me))
        def _():
            fin_copy(b).wait_send()


def attention(heads, parts, q, g, k, v, gate):
    blocks = heads * parts
    rows = k.shape[0]
    sub = rows // parts
    groups = blocks // parts
    vmem = pl.BlockSpec(memory_space=pltpu.VMEM)
    f32 = jnp.float32
    dma = pltpu.SemaphoreType.DMA
    wide = jax.ShapeDtypeStruct((rows, heads * HEAD), f32)
    return pl.pallas_call(
        lambda *refs: kernel_body(heads, parts, *refs),
        out_shape=(wide, jax.ShapeDtypeStruct((rows, heads * HEAD), LOW), wide, wide),
        in_specs=[vmem] * 5,
        out_specs=(vmem,) * 4,
        scratch_shapes=[
            pltpu.VMEM((blocks, 2, rows, HEAD), LOW),
            pltpu.VMEM((blocks, 2, sub, HEAD), LOW),
            pltpu.VMEM((blocks, 8, rows), f32),
            pltpu.VMEM((blocks, HEAD, rows), LOW),
            pltpu.VMEM((blocks, HEAD, rows), LOW),
            pltpu.VMEM((blocks, rows, HEAD), f32),
            pltpu.VMEM((blocks, rows, sub), f32),
            pltpu.VMEM((blocks, rows, HEAD), f32),
            pltpu.VMEM((blocks, rows, HEAD), f32),
            pltpu.VMEM((blocks, sub, HEAD), LOW),
            pltpu.VMEM((blocks, 2, rows, HEAD), LOW),
            pltpu.VMEM((groups, parts, 2, rows, HEAD), LOW),
            pltpu.VMEM((groups, 2, rows, HEAD), LOW),
            pltpu.VMEM((heads, parts, sub, HEAD), LOW),
            pltpu.VMEM((heads, 2, rows, HEAD), LOW),
            dma((blocks, 2)), dma((blocks, 2)), dma((blocks,)),
            dma((heads, 2)), dma((heads, parts, 2)), dma((heads, parts)), dma((heads, parts, 2)),
            dma((blocks,)), dma((blocks,)), dma((blocks,)), dma((groups, parts)),
            dma((groups,)), dma((heads,)), dma((5,)),
        ],
        compiler_params=pltpu.CompilerParams(
            vmem_limit_bytes=60 * 1024 * 1024, collective_id=0, has_side_effects=True
        ),
        cost_estimate=pl.CostEstimate(
            flops=12 * blocks * blocks * rows * sub * HEAD, bytes_accessed=1 << 22, transcendentals=0
        ),
        name="attention",
    )(q, g, k, v, gate)


def local(queries, keys, values, forget_logits, layer_input, out_grad):
    rows = queries.shape[0]
    heads = queries.shape[1] // HEAD
    parts = lax.axis_size("sp") // heads

    input_whole = lax.all_gather(layer_input, "tp", axis=1, tiled=True)
    gates = jnp.cumsum(jax.nn.log_sigmoid(forget_logits), axis=0).T * LOG2E
    totals = jnp.broadcast_to(gates[:, None, rows - 1 :], (heads, 7, rows))
    gates = jnp.concatenate([gates[:, None], totals], axis=1)
    query_grad, low, key_grad, value_grad = attention(
        heads, parts, queries, out_grad, keys, values, gates
    )
    weight_term = lax.dot_general(
        input_whole, low, (((0,), (0,)), ((), ())), preferred_element_type=jnp.float32
    )
    weight_grad = lax.psum_scatter(
        weight_term.astype(LOW), "sp", scatter_dimension=0, tiled=True
    ).astype(jnp.float32)
    return query_grad, key_grad, value_grad, weight_grad


def solution(mesh):
    spec = P("sp", "tp")
    return jax.shard_map(
        local, mesh=mesh, in_specs=(spec,) * 6, out_specs=(spec,) * 4, check_vma=False
    )
```

time: 332 us -> 253 us (0.76)
  blocking collectives: 100 us -> 0 us
  Pallas kernels: 41 us -> 135 us
  waiting for transfers between devices: 131 us -> 88.7 us
  starting transfers between devices: 15.7 us -> 0.08 us
  local copies, waits for them, and re-layouts: 13.7 us -> 5.55 us
  other arithmetic: 8.81 us -> 2.84 us
    all_gather x1 -> x0, blocking collectives: 100 us -> none  [local(): per_shard = lax.all_gather(local_gates, 'sp', axis=0)]
    all_to_all x3 -> x0, waiting for transfers between devices: 94.6 us -> none  [the longest x1 80.2 us: local(): both = lax.all_to_all(jnp.concatenate([dk, dv], axis=1), 'sp', 0, 0)]
    pallas_call x1, Pallas kernels: 41 us -> 135 us  [attention(): pl.pallas_call(lambda *refs: kernel_body(heads, parts, *refs), out_shape=...]
    reduce_scatter x1, waiting for transfers between devices: 35.5 us -> 88 us  [local(): lax.psum_scatter(weight_term.astype(LOW), 'sp', scatter_dimension=0, tile...]
    all_to_all x3 -> x0, starting transfers between devices: 15.6 us -> none  [the longest x1 7.41 us: local(): got = lax.all_to_all(packed, 'sp', 0, 0)]
    slice x6 -> x1, local copies, waits for them, and re-layouts: 3.49 us -> 0.16 us  [the longest x1 1.46 us: local(): k, v = (got[:, :rows], got[:, rows:2 * rows])]
  transfers between devices with their start and end apart: 5 -> 2, of which waited for: 3 -> 1; matrix products, arithmetic and copies ran while one was open for 4% -> 1% of each run, Pallas kernels for 12% -> 53%
where the time goes in v2:
time: 253 us
  Pallas kernels  135 us (53%)
  waiting for transfers between devices  88.7 us (35%)
  between operations  14.1 us (6%)
  matrix products  6.7 us (3%)
  local copies, waits for them, and re-layouts  5.55 us (2%)
  other arithmetic  2.84 us (1%)
    pallas_call x1, Pallas kernels, attention(): pl.pallas_call(lambda *refs: kernel_body(heads, parts, *refs), out_shape=...  135 us
    reduce_scatter x1, waiting for transfers between devices, local(): lax.psum_scatter(weight_term.astype(LOW), 'sp', scatter_dimension=0, tile...  88 us
    dot_general x1, matrix products, local(): lax.dot_general(input_whole, low, (((0,), (0,)), ((), ())), preferred_ele...  6.7 us
    unnamed x10, local copies, waits for them, and re-layouts  5.14 us
  transfers between devices with their start and end apart: 2, of which 1 were waited for; matrix products, arithmetic and copies ran while one was open for 1% of the time, Pallas kernels for 53%

profile of v2, /device:TPU:0, one launch (start us, length us, event | category | flops | bytes accessed | tf_op | source)
XLA Modules:
  0.0 252.7 jit_solution(15823461375917974796)
XLA Ops:
  7.2 0.0 all-gather.2.cloned.1.call-start
  7.2 0.7 all-gather.2.cloned.1.call-update
  7.9 0.0 reduce-scatter.2.cloned.1.call-start
  7.9 0.7 fusion.2
  8.7 1.2 reduce-window.6
  9.9 0.2 slice_reduce_fusion
  10.1 0.2 reduce-window.9
  10.3 0.1 add_multiply_fusion
  10.3 0.2 copy.14
  10.5 0.1 broadcast_in_dim.10
  10.6 0.6 pad_maximum_fusion.refs_4_
  11.2 134.7 %attention.1 = (f32[512,512]{1,0:T(8,128)}, bf16[512,512]{1,0:T(8,128)(2,1)}, f32[512,512]{1,0:T(8,128)}, f32[512,512]{1,0:T(8,128)}) custom-call(bf16[512,512]{1,0:T(8,128)(2,1)} %refs_0_.1, bf16[512,512]{1,0:T(8,128)(2,1)} %refs_1_.1, bf16[512,512]{1,0:T(8,128)(2,1)} %refs_2_.1, bf16[512,512]{1,0:T(8,128)(2,1)} %refs_3_.1, ...), custom_call_target="tpu_custom_call" | custom-call | flops 12884901888 | bytes 4194304 | tf_op jit(solution)/shard_map/attention/pallas_call | solution.py:309
  145.9 0.0 all-gather.2.cloned.1.call-done
  146.0 6.7 %fusion = bf16[4096,512]{0,1:T(8,128)(2,1)} fusion(bf16[512,512]{1,0:T(8,128)(2,1)} %get-tuple-element.11, bf16[512,4096]{1,0:T(8,128)(2,1)} %all-gather.2.cloned.1.call-done), kind=kOutput, calls=%fused_computation.1 | convolution fusion | flops 2149580800 | bytes 8912896 | tf_op jit(solution)/shard_map/dot_general | solution.py:357
  152.7 0.0 copy-start.2
  152.7 0.0 copy-start.1
  152.7 0.0 copy-start
  152.7 0.0 reduce-scatter.2.cloned.1.call-update
  152.7 88.0 %reduce-scatter.2.cloned.1.call-done = bf16[512,512]{0,1:T(8,128)(2,1)} async-done(((bf16[4096,512]{0,1:T(8,128)(2,1)}), bf16[512,512]{0,1:T(8,128)(2,1)}) %reduce-scatter.2.cloned.1.call-update) | async-done | bytes 524304 | tf_op jit(solution)/shard_map/reduce_scatter | solution.py:360
  240.7 2.2 copy.13
  242.9 0.0 copy-done.2
  242.9 1.0 copy.18
  243.9 0.0 copy-done.1
  243.9 1.0 copy.19
  244.9 0.0 copy-done
  244.9 1.0 copy.20
  (2 shorter events, 0.0 us)
Async XLA Ops:
  7.2 138.8 %all-gather.2.cloned.1.call-start = ((), (), s32[]{:S(2)}) async-start(), calls=%async_computation.1 | async-start | bytes 5242880 | tf_op jit(solution)/shard_map/all_gather | solution.py:350
  7.9 232.8 %reduce-scatter.2.cloned.1.call-start = ((), (), s32[]{:S(2)}) async-start(), calls=%async_computation.2 | async-start | bytes 4718592 | tf_op jit(solution)/shard_map/reduce_scatter | solution.py:360
  152.7 90.3 %copy-start.2 = (f32[512,512]{1,0:T(8,128)S(1)}, f32[512,512]{1,0:T(8,128)}, u32[]{:S(2)}) copy-start(f32[512,512]{1,0:T(8,128)} %get-tuple-element.24) | copy-start | bytes 3145732
  152.7 91.2 %copy-start.1 = (f32[512,512]{1,0:T(8,128)S(1)}, f32[512,512]{1,0:T(8,128)}, u32[]{:S(2)}) copy-start(f32[512,512]{1,0:T(8,128)} %get-tuple-element.25) | copy-start | bytes 3145732
  152.7 92.2 %copy-start = (f32[512,512]{1,0:T(8,128)S(1)}, f32[512,512]{1,0:T(8,128)}, u32[]{:S(2)}) copy-start(f32[512,512]{1,0:T(8,128)} %get-tuple-element.26) | copy-start | bytes 3145732
Sparse Core Ops, SparseCore 0:
  9.5 37.1 all-gather.1
  152.8 87.8 reduce-scatter.1

commit v3 on v2

--- a/solution.py
+++ b/solution.py
@@ -20,16 +20,20 @@
 
 
 def kernel_body(
-    heads, parts,
-    q_in, g_in, k_in, v_in, gate_in,
-    dq_out, low_out, dk_out, dv_out,
+    heads, parts, wide,
+    q_in, g_in, k_in, v_in, gate_in, x_in,
+    dq_out, dk_out, dv_out, w_out,
     kv, qg, gates, kt, vt, bias, sc, dk, dv, dq_stage, part_stage, red, fin, dq_got, kv_got,
+    x_all, low, w_stage, w_red, w_fin, w_got,
     kv_recv, qg_recv, gate_recv, kv_send, qg_send, gate_send, relay_send,
     dq_send, dq_recv, part_send, red_recv, fin_send, fin_recv, local_sem,
+    x_send, x_recv, w_send, w_recv, w_fin_send, w_fin_recv,
 ):
     blocks, _, rows, _ = kv.shape
     sub = qg.shape[2]
-    per_part = blocks // parts
+    span = w_out.shape[0]
+    x_width = x_in.shape[1]
+    column = lax.axis_index("tp")
     me = lax.axis_index("sp")
     head = me // parts
     part = lax.rem(me, parts)
@@ -42,7 +46,9 @@
     barrier = pltpu.get_barrier_semaphore()
     for r in range(1, blocks):
         pl.semaphore_signal(barrier, inc=1, device_id={"sp": lax.rem(me + r, blocks)})
-    pl.semaphore_wait(barrier, blocks - 1)
+    for r in range(1, wide):
+        pl.semaphore_signal(barrier, inc=1, device_id={"tp": lax.rem(column + r, wide)})
+    pl.semaphore_wait(barrier, blocks + wide - 2)
 
     def lanes(h):
         return pl.ds(pl.multiple_of(h * HEAD, HEAD), HEAD)
@@ -95,8 +101,21 @@
     ]
     own += [pltpu.make_async_copy(q_source(0, 0, i), qg.at[me, i], local_sem.at[2 + i]) for i in range(2)]
     own += [pltpu.make_async_copy(gate_in.at[head], gates.at[me], local_sem.at[4])]
+    own += [pltpu.make_async_copy(x_in, x_all.at[column], local_sem.at[5])]
     for copy in own:
         copy.start()
+
+    def x_copy(r, source):
+        return pltpu.make_async_remote_copy(
+            src_ref=x_in,
+            dst_ref=x_all.at[source],
+            send_sem=x_send.at[r],
+            recv_sem=x_recv.at[source],
+            device_id={"tp": lax.rem(column + r, wide)},
+        )
+
+    for r in range(1, wide):
+        x_copy(r, column).start()
 
     def kv_wait(j):
         for i in range(2):
@@ -260,15 +279,70 @@
         ).wait_recv()
     for h in range(heads):
         for n in range(parts):
-            piece = dq_got[h, n]
-            low_out[n * sub : (n + 1) * sub, h * HEAD : (h + 1) * HEAD] = piece
-            dq_out[n * sub : (n + 1) * sub, h * HEAD : (h + 1) * HEAD] = piece.astype(jnp.float32)
+            low[n * sub : (n + 1) * sub, h * HEAD : (h + 1) * HEAD] = dq_got[h, n]
+    for r in range(1, wide):
+        x_copy(r, lax.rem(column + r, wide)).wait_recv()
+
+    def term(c):
+        begin = c * span
+        x = x_all[begin // x_width, :, pl.ds(pl.multiple_of(lax.rem(begin, x_width), span), span)]
+        return lax.dot_general(x, low[...], (((0,), (0,)), ((), ())), preferred_element_type=jnp.float32)
+
+    def w_copy(r, c):
+        h, other = place(r, c)
+        return remote(
+            w_stage.at[r, c], w_red.at[h, part], w_send.at[r, c], w_recv.at[h, part], head * parts + other
+        )
+
+    def w_fin_copy(r):
+        h, _ = place(r, 0)
+        return remote(w_fin.at[r], w_got.at[head], w_fin_send.at[r], w_fin_recv.at[head], h * parts + part)
+
+    order = list(range(1, heads)) + [0]
+    waiting = None
+    for r in order:
+        for c in range(1, parts):
+            h, other = place(r, c)
+            w_stage[r, c] = term(h * parts + other).astype(LOW)
+            if waiting is not None:
+                waiting.start()
+            waiting = w_copy(r, c)
+    dq_out[...] = low[...].astype(jnp.float32)
+    if waiting is not None:
+        waiting.start()
+    waiting = None
+    for r in order:
+        h, _ = place(r, 0)
+        w_out[...] = term(h * parts + part)
+        if waiting is not None:
+            waiting.start()
+            waiting = None
+        for c in range(1, parts):
+            other = place(r, c)[1]
+            remote(
+                w_red.at[h, other], w_red.at[h, other], w_send.at[0, 0], w_recv.at[h, other], me
+            ).wait_recv()
+            w_out[...] += w_red[h, other].astype(jnp.float32)
+        if r:
+            w_fin[r] = w_out[...].astype(LOW)
+            waiting = w_fin_copy(r)
     for r in range(1, heads):
         h, _ = place(r, 0)
         remote(kv_got.at[h], kv_got.at[h], fin_send.at[0], fin_recv.at[h], me).wait_recv()
     for h in range(heads):
         dk_out[:, h * HEAD : (h + 1) * HEAD] = kv_got[h, 0].astype(jnp.float32)
         dv_out[:, h * HEAD : (h + 1) * HEAD] = kv_got[h, 1].astype(jnp.float32)
+    for r in range(1, heads):
+        h, _ = place(r, 0)
+        remote(w_got.at[h], w_got.at[h], w_fin_send.at[0], w_fin_recv.at[h], me).wait_recv()
+        w_out[...] += w_got[h].astype(jnp.float32)
+    for r in range(1, wide):
+        x_copy(r, column).wait_send()
+    for r in range(heads):
+        for c in range(1, parts):
+            w_copy(r, c).wait_send()
+    for r in range(1, heads):
+        w_fin_copy(r).wait_send()
 
     for r in range(1, heads):
         for i in range(2):
@@ -297,7 +371,7 @@
             fin_copy(b).wait_send()
 
 
-def attention(heads, parts, q, g, k, v, gate):
+def attention(heads, parts, wide, q, g, k, v, gate, x):
     blocks = heads * parts
     rows = k.shape[0]
     sub = rows // parts
@@ -305,11 +379,13 @@
     vmem = pl.BlockSpec(memory_space=pltpu.VMEM)
     f32 = jnp.float32
     dma = pltpu.SemaphoreType.DMA
-    wide = jax.ShapeDtypeStruct((rows, heads * HEAD), f32)
+    cols = heads * HEAD
+    span = x.shape[1] * wide // blocks
+    grad = jax.ShapeDtypeStruct((rows, cols), f32)
     return pl.pallas_call(
-        lambda *refs: kernel_body(heads, parts, *refs),
-        out_shape=(wide, jax.ShapeDtypeStruct((rows, heads * HEAD), LOW), wide, wide),
-        in_specs=[vmem] * 5,
+        lambda *refs: kernel_body(heads, parts, wide, *refs),
+        out_shape=(grad, grad, grad, jax.ShapeDtypeStruct((span, cols), f32)),
+        in_specs=[vmem] * 6,
         out_specs=(vmem,) * 4,
         scratch_shapes=[
             pltpu.VMEM((blocks, 2, rows, HEAD), LOW),
@@ -327,10 +403,17 @@
             pltpu.VMEM((groups, 2, rows, HEAD), LOW),
             pltpu.VMEM((heads, parts, sub, HEAD), LOW),
             pltpu.VMEM((heads, 2, rows, HEAD), LOW),
+            pltpu.VMEM((wide, rows, x.shape[1]), LOW),
+            pltpu.VMEM((rows, cols), LOW),
+            pltpu.VMEM((heads, parts, span, cols), LOW),
+            pltpu.VMEM((heads, parts, span, cols), LOW),
+            pltpu.VMEM((heads, span, cols), LOW),
+            pltpu.VMEM((heads, span, cols), LOW),
             dma((blocks, 2)), dma((blocks, 2)), dma((blocks,)),
             dma((heads, 2)), dma((heads, parts, 2)), dma((heads, parts)), dma((heads, parts, 2)),
             dma((blocks,)), dma((blocks,)), dma((blocks,)), dma((groups, parts)),
-            dma((groups,)), dma((heads,)), dma((5,)),
+            dma((groups,)), dma((heads,)), dma((6,)),
+            dma((wide,)), dma((wide,)), dma((heads, parts)), dma((heads, parts)), dma((heads,)), dma((heads,)),
         ],
         compiler_params=pltpu.CompilerParams(
             vmem_limit_bytes=60 * 1024 * 1024, collective_id=0, has_side_effects=True
@@ -339,7 +422,7 @@
             flops=12 * blocks * blocks * rows * sub * HEAD, bytes_accessed=1 << 22, transcendentals=0
         ),
         name="attention",
-    )(q, g, k, v, gate)
+    )(q, g, k, v, gate, x)
 
 
 def local(queries, keys, values, forget_logits, layer_input, out_grad):
@@ -347,20 +430,13 @@
     heads = queries.shape[1] // HEAD
     parts = lax.axis_size("sp") // heads
 
-    input_whole = lax.all_gather(layer_input, "tp", axis=1, tiled=True)
+    wide = lax.axis_size("tp")
     gates = jnp.cumsum(jax.nn.log_sigmoid(forget_logits), axis=0).T * LOG2E
     totals = jnp.broadcast_to(gates[:, None, rows - 1 :], (heads, 7, rows))
     gates = jnp.concatenate([gates[:, None], totals], axis=1)
-    query_grad, low, key_grad, value_grad = attention(
-        heads, parts, queries, out_grad, keys, values, gates
+    return attention(
+        heads, parts, wide, queries, out_grad, keys, values, gates, layer_input
     )
-    weight_term = lax.dot_general(
-        input_whole, low, (((0,), (0,)), ((), ())), preferred_element_type=jnp.float32
-    )
-    weight_grad = lax.psum_scatter(
-        weight_term.astype(LOW), "sp", scatter_dimension=0, tiled=True
-    ).astype(jnp.float32)
-    return query_grad, key_grad, value_grad, weight_grad
 
 
 def solution(mesh):

time: 253 us -> 191 us (0.75)
  waiting for transfers between devices: 88.7 us -> 0 us
  Pallas kernels: 135 us -> 178 us
  between operations: 14.1 us -> 0.68 us
  matrix products: 6.7 us -> 0 us
    reduce_scatter x1 -> x0, waiting for transfers between devices: 88 us -> none  [local(): lax.psum_scatter(weight_term.astype(LOW), 'sp', scatter_dimension=0, tile...]
    pallas_call x1, Pallas kernels: 135 us -> 178 us  [attention(): pl.pallas_call(lambda *refs: kernel_body(heads, parts, wide, *refs), out_...]
    dot_general x1 -> x0, matrix products: 6.7 us -> none  [local(): lax.dot_general(input_whole, low, (((0,), (0,)), ((), ())), preferred_ele...]
  transfers between devices with their start and end apart: 2 -> 0, of which waited for: 1 -> 0; matrix products, arithmetic and copies ran while one was open for 1% -> 0% of each run, Pallas kernels for 53% -> 0%
where the time goes in v3:
time: 191 us; the launch traced here: 189 us
  Pallas kernels  178 us (93%)
  local copies, waits for them, and re-layouts  6.93 us (4%)
  other arithmetic  2.85 us (1%)
    pallas_call x1, Pallas kernels, attention(): pl.pallas_call(lambda *refs: kernel_body(heads, parts, wide, *refs), out_...  178 us
    unnamed x10, local copies, waits for them, and re-layouts  6.53 us

profile of v3, /device:TPU:0, one launch (start us, length us, event | category | flops | bytes accessed | tf_op | source)
XLA Modules:
  0.0 188.6 jit_solution(5744799041618510082)
XLA Ops:
  0.6 0.7 fusion.1
  1.4 1.2 reduce-window.6
  2.6 0.2 slice_reduce_fusion
  2.8 0.2 reduce-window.9
  2.9 0.1 add_multiply_fusion
  3.0 0.2 copy.12
  3.2 0.1 broadcast_in_dim.10
  3.3 0.7 pad_maximum_fusion.refs_4_
  3.9 178.1 %attention.1 = (f32[512,512]{1,0:T(8,128)}, f32[512,512]{1,0:T(8,128)}, f32[512,512]{1,0:T(8,128)}, f32[512,512]{1,0:T(8,128)}) custom-call(bf16[512,512]{1,0:T(8,128)(2,1)} %refs_0_.1, bf16[512,512]{1,0:T(8,128)(2,1)} %refs_1_.1, bf16[512,512]{1,0:T(8,128)(2,1)} %refs_2_.1, bf16[512,512]{1,0:T(8,128)(2,1)} %refs_3_.1, ...), custom_call_target="tpu_custom_call" | custom-call | flops 12884901888 | bytes 4194304 | tf_op jit(solution)/shard_map/attention/pallas_call | solution.py:385
  182.0 0.0 copy-start.2
  182.0 2.4 %copy.17 = f32[512,512]{1,0:T(8,128)} copy(f32[512,512]{1,0:T(8,128)} %get-tuple-element.8) | data formatting | bytes 2097152
  184.4 0.0 copy-done.2
  184.4 0.0 copy-start.1
  184.4 1.0 copy.18
  185.4 0.6 copy-done.1
  186.0 0.0 copy-start
  186.0 1.0 copy.19
  187.0 0.6 copy-done
  187.6 1.0 copy.20
  (2 shorter events, 0.0 us)
Async XLA Ops:
  182.0 2.4 %copy-start.2 = (f32[512,512]{1,0:T(8,128)S(1)}, f32[512,512]{1,0:T(8,128)}, u32[]{:S(2)}) copy-start(f32[512,512]{1,0:T(8,128)} %get-tuple-element.9) | copy-start | bytes 3145732
  184.4 1.6 copy-start.1
  186.0 1.6 copy-start

commit v4 on v3

--- a/solution.py
+++ b/solution.py
@@ -121,30 +121,38 @@
         for i in range(2):
             remote(kv.at[j, i], kv.at[j, i], kv_send.at[0, i], kv_recv.at[j, i], me).wait_recv()
 
+    def turn(j):
+        kt[j] = kv[j, 0].T
+        vt[j] = kv[j, 1].T
+
+    @pl.loop(0, blocks)
+    def _(j):
+        dk[j] = jnp.zeros((rows, HEAD), jnp.float32)
+        dv[j] = jnp.zeros((rows, HEAD), jnp.float32)
+
+    for copy in own:
+        copy.wait()
+    turn(me)
     for r in range(1, heads):
         j = place(r, 0)[0] * parts + part
         kv_wait(j)
         for c in range(1, parts):
             for i in range(2):
                 relay_copy(r, c, i).start()
-    for copy in own:
-        copy.wait()
+        turn(j)
     for r, c in pairs:
         h, other = place(r, c)
         j = h * parts + other
         if c:
             kv_wait(j)
+            turn(j)
         for i in range(2):
             remote(qg.at[j, i], qg.at[j, i], qg_send.at[0, 0, i], qg_recv.at[j, i], me).wait_recv()
         remote(gates.at[j], gates.at[j], gate_send.at[0, 0], gate_recv.at[j], me).wait_recv()
 
     def prepare(j, base):
-        kt[j] = kv[j, 0].T
-        vt[j] = kv[j, 1].T
         row = gates[j, 0:1] + base
         bias[j] = jnp.broadcast_to(row, (HEAD, rows)).T
-        dk[j] = jnp.zeros((rows, HEAD), jnp.float32)
-        dv[j] = jnp.zeros((rows, HEAD), jnp.float32)
         return base + gates[j, 1:2]
 
     lax.fori_loop(0, blocks, prepare, jnp.zeros((1, rows), jnp.float32))

time: 191 us -> 190 us (level)
  no operation moved by 1% of the time
where the time goes in v4:
time: 190 us; the launch traced here: 188 us
  Pallas kernels  178 us (94%)
  local copies, waits for them, and re-layouts  6.93 us (4%)
  other arithmetic  2.85 us (2%)
    pallas_call x1, Pallas kernels, attention(): pl.pallas_call(lambda *refs: kernel_body(heads, parts, wide, *refs), out_...  178 us
    unnamed x10, local copies, waits for them, and re-layouts  6.53 us

profile of v4, /device:TPU:0, one launch (start us, length us, event | category | flops | bytes accessed | tf_op | source)
XLA Modules:
  0.0 188.2 jit_solution(12721201292961593831)
XLA Ops:
  0.6 0.7 fusion.1
  1.4 1.2 reduce-window.6
  2.6 0.2 slice_reduce_fusion
  2.8 0.2 reduce-window.9
  2.9 0.1 add_multiply_fusion
  3.0 0.2 copy.12
  3.2 0.1 broadcast_in_dim.10
  3.3 0.7 pad_maximum_fusion.refs_4_
  3.9 177.7 %attention.1 = (f32[512,512]{1,0:T(8,128)}, f32[512,512]{1,0:T(8,128)}, f32[512,512]{1,0:T(8,128)}, f32[512,512]{1,0:T(8,128)}) custom-call(bf16[512,512]{1,0:T(8,128)(2,1)} %refs_0_.1, bf16[512,512]{1,0:T(8,128)(2,1)} %refs_1_.1, bf16[512,512]{1,0:T(8,128)(2,1)} %refs_2_.1, bf16[512,512]{1,0:T(8,128)(2,1)} %refs_3_.1, ...), custom_call_target="tpu_custom_call" | custom-call | flops 12884901888 | bytes 4194304 | tf_op jit(solution)/shard_map/attention/pallas_call | solution.py:393
  181.6 0.0 copy-start.2
  181.6 2.4 %copy.17 = f32[512,512]{1,0:T(8,128)} copy(f32[512,512]{1,0:T(8,128)} %get-tuple-element.8) | data formatting | bytes 2097152
  184.0 0.0 copy-done.2
  184.0 0.0 copy-start.1
  184.0 1.0 copy.18
  185.0 0.6 copy-done.1
  185.6 0.0 copy-start
  185.6 1.0 copy.19
  186.6 0.6 copy-done
  187.2 1.0 copy.20
  (2 shorter events, 0.0 us)
Async XLA Ops:
  181.6 2.4 %copy-start.2 = (f32[512,512]{1,0:T(8,128)S(1)}, f32[512,512]{1,0:T(8,128)}, u32[]{:S(2)}) copy-start(f32[512,512]{1,0:T(8,128)} %get-tuple-element.9) | copy-start | bytes 3145732
  184.0 1.6 copy-start.1
  185.6 1.6 copy-start
